TPU v7x, 128 devices: a whole 4x4x4 slice. The times are simulated.
128 devices in a mesh: sp: 16 (over z, y), tp: 8 (over x, core).
Axes of the slice: x: 4, y: 4, z: 4, core: 2. Of those that a mesh axis runs over, the one named last changes fastest.
Arguments:
- skip_stream_vector: bfloat16 [16384, 2048], P(('sp', 'tp')), may hold values from -6 to 6
- probe_preactivation: bfloat16 [16384, 1024], P('sp', 'tp'), may hold values from -6 to 6
- retention_preactivation: bfloat16 [16384, 1024], P('sp', 'tp'), may hold values from -4.5 to 4.5
- content_vector: bfloat16 [16384, 1024], P('sp', 'tp'), may hold values from -6 to 6
- emission_preactivation: bfloat16 [16384, 1024], P('sp', 'tp'), may hold values from -6 to 6
- retention_slack: float32 [1024], P('tp'), may hold values from 0 to 0.12
- surge_rate: float32 [16384, 1024], P('sp', 'tp'), may hold values from -1.2 to 0
- subspace_scaling_factor: float32 [1024], P('tp'), may hold values from 0.1 to 1.9
- emission_matrix: bfloat16 [1024, 2048], replicated, may hold values from -0.1875 to 0.1875
- mlp_scaling_factor: float32 [2048], replicated, may hold values from 0.1 to 1.9
- switch_matrix: bfloat16 [2048, 5632], P('sp', 'tp'), may hold values from -0.125 to 0.125
- expansion_matrix: bfloat16 [2048, 5632], P('sp', 'tp'), may hold values from -0.125 to 0.125
- contraction_matrix: bfloat16 [5632, 2048], P('tp', 'sp'), may hold values from -0.078125 to 0.078125
Outputs:
- stream_out: bfloat16 [16384, 2048], P(('sp', 'tp'))
All inputs are finite; a program needn't handle non-finite values.
Results may differ from a plain program's by a relative error of at most 0.017.
Values may be sent and summed in bfloat16 or wider, within the bound.
A program may use at most 128 MiB of HBM per device.

v0:
```python
import jax
import jax.numpy as jnp
from jax import lax
from jax.sharding import Mesh
from jax.sharding import PartitionSpec as P

HEAD_DIM = 128
BLOCK = 64
TP = ("tp_0", "tp_1")
SP_TP = ("sp", "tp_0", "tp_1")
EPSILON = 1e-06
TOP_PRECISION = lax.Precision.HIGHEST


def in_one_piece(arrays, axis, dim, along):
    both = jnp.concatenate(arrays, axis=along)
    whole, at, outs = (lax.all_gather(both, axis, axis=dim, tiled=True), 0, [])
    for a in arrays:
        outs.append(lax.slice_in_dim(whole, at, at + a.shape[along], axis=along))
        at += a.shape[along]
    return tuple(outs)


def from_everyone(value, axis):
    peers = lax.axis_size(axis)
    return lax.all_to_all(
        jnp.broadcast_to(value[None], (peers, *value.shape)), axis, 0, 0, tiled=True
    )


def all_in_one(value, axis):
    leaves = jax.tree.leaves(value)
    order = sorted(range(len(leaves)), key=lambda k: -leaves[k].size)
    width = (1, *leaves[order[0]].shape)[-1]
    lines = [
        jnp.pad(leaves[k].reshape(-1), (0, -leaves[k].size % width)).reshape(-1, width)
        for k in order
    ]
    both, at, found = (from_everyone(jnp.concatenate(lines), axis), 0, {})
    for k, line in zip(order, lines):
        piece = both[:, at : at + len(line)].reshape(len(both), -1)
        found[k] = piece[:, : leaves[k].size].reshape(-1, *leaves[k].shape)
        at += len(line)
    numbers = iter(range(len(leaves)))
    return jax.tree.map(lambda _: found[next(numbers)], value)


def joined_by_halves(pieces, combine):
    while len(jax.tree.leaves(pieces)[0]) > 1:
        pieces = jax.vmap(combine)(
            *(jax.tree.map(lambda part: part[side::2], pieces) for side in (0, 1))
        )
    return jax.tree.map(lambda part: part[0], pieces)


def carried_in(value, axis, combine, identity):
    peers, here = (lax.axis_size(axis), lax.axis_index(axis))
    passed = jnp.arange(peers) < here

    def kept(part, zero, own):
        part = jnp.where(
            passed.reshape(-1, *(1 for _ in own.shape)),
            part.astype(own.dtype),
            jnp.asarray(zero, own.dtype),
        )
        return part

    pieces = all_in_one(
        jax.tree.map(lambda part, kind: part.astype(kind), value, (jnp.bfloat16, jnp.bfloat16)),
        axis,
    )
    return joined_by_halves(jax.tree.map(kept, pieces, identity, value), combine)


def joined_along(tiles, dim):
    lengths = list(tiles.shape[1:])
    lengths[dim] *= tiles.shape[0]
    return jnp.moveaxis(tiles, 0, dim).reshape(lengths)


def gathered_by_axis(value, axes, dim):
    far, near = axes
    tiles = from_everyone(from_everyone(value, far), near)
    return joined_along(tiles.swapaxes(0, 1).reshape(-1, *value.shape), dim)


def in_blocks(value, dim, peers):
    lengths = value.shape
    tiles = value.reshape(*lengths[:dim], peers, lengths[dim] // peers, *lengths[dim + 1 :])
    return jnp.moveaxis(tiles, dim, 0)


def summed_on_arrival(value, axis, dim):
    tiles = in_blocks(value, dim, lax.axis_size(axis))
    arrived = lax.all_to_all(tiles, axis, split_axis=0, concat_axis=0, tiled=True)
    return arrived.astype(jnp.float32).sum(axis=0)


def sum_by_axis(value, axes, dim):
    far, near = axes
    own = summed_on_arrival(in_blocks(value, dim, lax.axis_size(far)), near, dim + 1)
    return jnp.sum(
        lax.all_to_all(own.astype(jnp.bfloat16), far, 0, 0, tiled=True).astype(jnp.float32), axis=0
    )


def block_step(carry, inputs):
    memory_state, offsets = carry
    query_block, input_gate_block, value_block, log_blk = inputs
    cumulative_decay = jnp.cumsum(log_blk, axis=1)
    length = log_blk.shape[1]
    carried_share = jnp.einsum(
        "eia,eax->eix",
        query_block * jnp.exp(cumulative_decay),
        memory_state,
        precision=TOP_PRECISION,
    )
    middle = cumulative_decay[:, length // 2, :][:, None, :]
    left_side = query_block * jnp.exp(cumulative_decay - middle)
    right_side = input_gate_block * jnp.exp(middle - cumulative_decay)
    causal = (jnp.arange(length)[:, None] >= jnp.arange(length)[None, :])[None, :, :]
    scores = jnp.einsum("htk,hsk->hts", left_side, right_side, precision=TOP_PRECISION)
    scores = jnp.where(causal, scores, 0.0)
    outputs = carried_share + jnp.einsum(
        "hts,hsv->htv", scores, value_block, precision=TOP_PRECISION
    )
    closing_log_decay = cumulative_decay[:, -1, :]
    updated_memory_state = jnp.exp(closing_log_decay)[:, :, None] * memory_state + jnp.einsum(
        "qnj,qnl->qjl",
        input_gate_block * jnp.exp(closing_log_decay[:, None, :] - cumulative_decay),
        value_block,
        precision=TOP_PRECISION,
    )
    return (
        (updated_memory_state, offsets + closing_log_decay),
        (outputs, cumulative_decay + offsets[:, None, :]),
    )


def split_blocks(values, heads_here):
    count = values.shape[0]
    return values.reshape(count // BLOCK, BLOCK, heads_here, HEAD_DIM).transpose(0, 2, 1, 3)


def admission_source_matrix(
    probe_preactivation, retention_preactivation, content_vector, retention_slack, surge_rate
):
    query_act = jax.nn.silu(probe_preactivation.astype(jnp.float32))
    admission_factor = retention_slack[None, :] * jax.nn.sigmoid(
        -retention_preactivation.astype(jnp.float32)
    )
    retention_logarithm = jnp.log1p(-admission_factor) + surge_rate
    return (query_act, admission_factor, content_vector.astype(jnp.float32), retention_logarithm)


def head_output(outputs, subspace_scaling_factor, emission_preactivation):
    count, heads_here = (outputs.shape[0], outputs.shape[1])
    squares = jnp.mean(outputs * outputs, axis=-1, keepdims=True)
    scaled = (
        outputs
        * lax.rsqrt(squares + EPSILON)
        * subspace_scaling_factor.reshape(heads_here, HEAD_DIM)
    )
    scaled = scaled.reshape(count, heads_here * HEAD_DIM)
    return (scaled * jax.nn.silu(emission_preactivation.astype(jnp.float32))).astype(jnp.bfloat16)


def row_norm(stream, mlp_scaling_factor):
    streamf = stream.astype(jnp.float32)
    squares = jnp.mean(streamf * streamf, axis=-1, keepdims=True)
    return (streamf * lax.rsqrt(squares + EPSILON) * mlp_scaling_factor).astype(jnp.bfloat16)


def chain(earlier, later):
    return (earlier[0] * later[0], later[0][:, :, None] * earlier[1] + later[1])


def on_device(
    skip_stream_vector,
    probe_preactivation,
    retention_preactivation,
    content_vector,
    emission_preactivation,
    retention_slack,
    surge_rate,
    subspace_scaling_factor,
    emission_matrix,
    mlp_scaling_factor,
    switch_matrix,
    expansion_matrix,
    contraction_matrix,
):
    gate_whole, up_whole = in_one_piece((switch_matrix, expansion_matrix), "sp", 0, 1)
    down_whole = lax.all_gather(contraction_matrix, "sp", axis=1, tiled=True)
    heads_here = probe_preactivation.shape[1] // HEAD_DIM
    tok_rows = probe_preactivation.shape[0]
    arranged_sources = admission_source_matrix(
        probe_preactivation, retention_preactivation, content_vector, retention_slack, surge_rate
    )
    block_list = tuple((split_blocks(item, heads_here) for item in arranged_sources))
    start_carry = (
        jnp.zeros((heads_here, HEAD_DIM, HEAD_DIM), jnp.float32),
        jnp.zeros((heads_here, HEAD_DIM), jnp.float32),
    )
    (memory_state, offsets), (outputs, cumulative_log_decay) = lax.scan(
        block_step, start_carry, block_list
    )
    incoming_state = carried_in(
        (jnp.exp(offsets), memory_state),
        "sp",
        chain,
        (jnp.ones_like(offsets), jnp.zeros_like(memory_state)),
    )
    outputs = outputs + jnp.einsum(
        "jmxo,mos->jmxs",
        block_list[0] * jnp.exp(cumulative_log_decay),
        incoming_state[1],
        precision=TOP_PRECISION,
    )
    outputs = outputs.transpose(0, 2, 1, 3).reshape(tok_rows, heads_here, HEAD_DIM)
    mixed = head_output(outputs, subspace_scaling_factor, emission_preactivation)
    regrouped = lax.all_to_all(mixed, TP, split_axis=0, concat_axis=1, tiled=True)
    projected = jnp.dot(regrouped, emission_matrix, preferred_element_type=jnp.float32)
    stream = (skip_stream_vector.astype(jnp.float32) + projected).astype(jnp.bfloat16)
    normed = row_norm(stream, mlp_scaling_factor)
    all_rows = gathered_by_axis(normed, ("tp_0", "tp_1"), 0)
    gate_proj = jnp.dot(all_rows, gate_whole, preferred_element_type=jnp.float32)
    up_proj = jnp.dot(all_rows, up_whole, preferred_element_type=jnp.float32)
    hidden = (jax.nn.silu(gate_proj) * up_proj).astype(jnp.bfloat16)
    partial_sum = jnp.dot(hidden, down_whole, preferred_element_type=jnp.float32)
    summed = sum_by_axis(partial_sum.astype(jnp.bfloat16), ("tp_0", "tp_1"), 0)
    return (stream.astype(jnp.float32) + summed).astype(jnp.bfloat16)


def solution(mesh):
    split = Mesh(mesh.devices.reshape(mesh.shape["sp"], 4, 2), ("sp", "tp_0", "tp_1"))
    return jax.shard_map(
        on_device,
        mesh=split,
        in_specs=(
            P(SP_TP, None),
            P("sp", TP),
            P("sp", TP),
            P("sp", TP),
            P("sp", TP),
            P(TP),
            P("sp", TP),
            P(TP),
            P(),
            P(),
            P("sp", TP),
            P("sp", TP),
            P(TP, "sp"),
        ),
        out_specs=P(SP_TP, None),
        check_vma=False,
    )
```

profile of v0, /device:TPU:0, one launch (start us, length us, event | category | flops | bytes accessed | tf_op | source)
XLA Modules:
  0.0 193.7 jit_solution(10395686392634396452)
XLA Ops:
  6.5 1.8 pad_maximum_fusion
  8.4 1.1 convert_multiply_fusion.1
  9.5 1.0 convert.2
  10.5 1.5 divide_multiply_fusion
  12.0 17.0 %while.17 = (s32[]{:T(128)}, f32[1,128,128]{2,1,0:T(8,128)S(1)}, f32[1,128]{1,0:T(1,128)S(1)}, f32[16,1,64,128]{3,2,1,0:T(8,128)S(1)}, f32[16,1,64,128]{3,2,1,0:...) while((s32[]{:T(128)}, f32[1,128,128]{2,1,0:T(8,128)S(1)}, ...), condition=%wide.region_2.3_spmd.clone, body=%wide.region_0.2_spmd.clone.sunk | while | flops 38412544 | bytes 879768 | solution.py:205
  12.5 0.3 fusion.99
  13.6 0.3 fusion.99
  14.7 0.3 fusion.99
  15.7 0.3 fusion.99
  17.8 0.3 fusion.99
  18.9 0.3 fusion.99
  21.0 0.3 fusion.99
  29.0 0.9 broadcast_in_dim.48
  29.9 8.2 %all-to-all-start = ((bf16[16,129,128]{2,1,0:T(8,128)(2,1)}), bf16[16,129,128]{2,1,0:T(8,128)(2,1)S(1)}, u32[]{:S(2)}, u32[]{:S(2)}) async-start(bf16[16,129,128]{2,1,0:T(8,128)(2,1)} %broadcast_in_dim.48), calls=%async_computation | async-start | bytes 1114112 | tf_op jit(solution)/shard_map/all_to_all | solution.py:26
  38.1 0.7 all-gather.5.cloned.1.call-update
  38.9 11.2 %all-to-all-done = bf16[16,129,128]{2,1,0:T(8,128)(2,1)S(1)} async-done(((bf16[16,129,128]{2,1,0:T(8,128)(2,1)}), bf16[16,129,128]{2,1,0:T(8,128)(2,1)S(1)}, u32[]{:S(2)}, u32[]{:S(2)}) %all-to-all-start) | async-done | bytes 528416 | tf_op jit(solution)/shard_map/all_to_all | solution.py:26
  50.8 0.7 multiply_reduce_fusion.1
  51.9 11.6 %all_to_all.44 = bf16[8,128,128]{2,1,0:T(8,128)(2,1)S(1)} all-to-all(bf16[8,128,128]{2,1,0:T(8,128)(2,1)S(1)} %bitcast.185), channel_id=1, replica_groups=mesh['sp'=16,'tp_0'=4,'tp_1'=2] {'tp_0','tp_1'}, dimensions={0} | all-to-all | bytes 524288 | tf_op jit(solution)/shard_map/all_to_all | solution.py:222
  63.7 3.0 %multiply_reduce_fusion = (f32[128]{0:T(128)S(1)}, f32[128,2048]{1,0:T(8,128)S(1)}) fusion(bf16[128,1024]{0,1:T(8,128)(2,1)S(1)} %bitcast.183, bf16[1024,2048]{1,0:T(8,128)(2,1)} %param.23, bf16[128,2048]{1,0:T(8,128)(2,1)S(1)} %copy-done), kind=kOutput, calls=%fused_computation.66 | convolution fusion | flops 538443648 | bytes 6029824 | tf_op jit(solution)/shard_map/dot_general | solution.py:223
  67.1 28.8 %all_to_all.45 = bf16[4,128,2048]{2,1,0:T(8,128)(2,1)S(1)} all-to-all(bf16[4,128,2048]{2,1,0:T(8,128)(2,1)S(1)} %broadcast_in_dim.74), channel_id=1, replica_groups=mesh['sp'=16,'tp_0'=4,'tp_1'=2] {'tp_0'}, dimensions={0} | all-to-all | bytes 4194304 | tf_op jit(solution)/shard_map/all_to_all | solution.py:26
  95.9 0.5 broadcast_in_dim.75
  96.5 7.1 %all_to_all.46 = bf16[2,4,128,2048]{3,2,1,0:T(8,128)(2,1)S(1)} all-to-all(bf16[2,4,128,2048]{3,2,1,0:T(8,128)(2,1)S(1)} %broadcast_in_dim.75), channel_id=1, replica_groups=mesh['sp'=16,'tp_0'=4,'tp_1'=2] {'tp_1'}, dimensions={0} | all-to-all | bytes 8388608 | tf_op jit(solution)/shard_map/all_to_all | solution.py:26
  103.6 2.3 %copy.36 = bf16[2,4,128,2048]{3,2,0,1:T(8,128)(2,1)} copy(bf16[2,4,128,2048]{3,2,1,0:T(8,128)(2,1)S(1)} %all_to_all.46) | data formatting | bytes 8388608 | tf_op jit(solution)/shard_map/all_to_all | solution.py:26
  105.9 7.9 %fusion.43 = f32[1024,704]{0,1:T(8,128)} fusion(bf16[1024,2048]{1,0:T(8,128)(2,1)} %bitcast.178, bf16[2048,1408]{0,1:T(8,128)(2,1)} %all-gather.3.cloned.1.call-done), kind=kOutput, calls=%fused_computation.56 | convolution fusion | flops 2952790016 | bytes 9961472 | tf_op jit(solution)/shard_map/dot_general | solution.py:227
  113.8 14.8 %all-gather.5.cloned.1.call-done = bf16[704,2048]{1,0:T(8,128)(2,1)} async-done(((bf16[704,128]{1,0:T(8,128)(2,1)}), bf16[704,2048]{1,0:T(8,128)(2,1)}) %all-gather.5.cloned.1.call-update) | async-done | bytes 2883600 | tf_op jit(solution)/shard_map/all_gather | solution.py:194
  128.6 12.1 %convolution_convert_fusion = bf16[1024,2048]{1,0:T(8,128)(2,1)} fusion(bf16[704,2048]{1,0:T(8,128)(2,1)} %all-gather.5.cloned.1.call-done, f32[1024,704]{0,1:T(8,128)} %fusion.43, bf16[1024,2048]{1,0:T(8,128)(2,1)} %bitcast.179, bf16[2048,1408]{0,1:T(8,128)(2,1)} %all-gather.3.cloned.1.call-done), kind=kOutput, calls=%fused_computation.53 | convolution fusion | flops 5912002560 | bytes 17039360 | tf_op jit(solution)/shard_map/dot_general | solution.py:230
  140.7 2.5 %copy.39 = bf16[4,2,128,2048]{3,2,0,1:T(8,128)(2,1)S(1)} copy(bf16[4,2,128,2048]{3,2,1,0:T(8,128)(2,1)} %bitcast.180) | data formatting | bytes 8388608 | tf_op jit(solution)/shard_map/reshape;reshape | solution.py:89
  143.2 8.2 %all_to_all.47 = bf16[2,4,128,2048]{3,2,1,0:T(8,128)(2,1)} all-to-all(bf16[2,4,128,2048]{3,2,1,0:T(8,128)(2,1)S(1)} %bitcast.177), channel_id=1, replica_groups=mesh['sp'=16,'tp_0'=4,'tp_1'=2] {'tp_1'}, dimensions={0} | all-to-all | bytes 8388608 | tf_op jit(solution)/shard_map/all_to_all | solution.py:95
  151.3 3.5 %reduce_sum.41 = bf16[4,128,2048]{2,1,0:T(8,128)(2,1)S(1)} reduce(bf16[2,4,128,2048]{3,2,1,0:T(8,128)(2,1)} %all_to_all.47, bf16[]{:T(256)} %constant.49.clone.1), dimensions={0}, to_apply=%region_5.6 | reduce | flops 1048576 | bytes 6291458 | tf_op jit(solution)/shard_map/reduce_sum | solution.py:96
  154.9 30.7 %all_to_all.48 = bf16[4,128,2048]{2,1,0:T(8,128)(2,1)S(1)} all-to-all(bf16[4,128,2048]{2,1,0:T(8,128)(2,1)S(1)} %reduce_sum.41), channel_id=1, replica_groups=mesh['sp'=16,'tp_0'=4,'tp_1'=2] {'tp_0'}, dimensions={0} | all-to-all | bytes 4194304 | tf_op jit(solution)/shard_map/all_to_all | solution.py:103
  185.6 0.4 convert_reduce_fusion
  186.0 0.9 add_convert_fusion
  (189 shorter events, 15.5 us)
Async XLA Ops:
  6.5 99.4 %all-gather.3.cloned.1.call-start = ((), (), s32[]{:S(2)}) async-start(), calls=%async_computation.6 | async-start | bytes 6127616 | tf_op jit(solution)/shard_map/all_gather | solution.py:17
  29.9 20.2 %all-to-all-start = ((bf16[16,129,128]{2,1,0:T(8,128)(2,1)}), bf16[16,129,128]{2,1,0:T(8,128)(2,1)S(1)}, u32[]{:S(2)}, u32[]{:S(2)}) async-start(bf16[16,129,128]{2,1,0:T(8,128)(2,1)} %broadcast_in_dim.48), calls=%async_computation | async-start | bytes 1114112 | tf_op jit(solution)/shard_map/all_to_all | solution.py:26
  38.1 90.5 %all-gather.5.cloned.1.call-start = ((), (), s32[]{:S(2)}) async-start(), calls=%async_computation.7 | async-start | bytes 3063808 | tf_op jit(solution)/shard_map/all_gather | solution.py:194
  50.3 1.3 copy-start.1
  50.3 1.3 copy-start.3
  50.6 13.1 %copy-start = (bf16[128,2048]{1,0:T(8,128)(2,1)S(1)}, bf16[128,2048]{1,0:T(8,128)(2,1)}, u32[]{:S(2)}) copy-start(bf16[128,2048]{1,0:T(8,128)(2,1)} %param.15) | copy-start | bytes 1572868
  63.7 3.0 %copy-start.2 = (f32[2048]{0:T(1024)S(1)}, f32[2048]{0:T(1024)}, u32[]{:S(2)}) copy-start(f32[2048]{0:T(1024)} %param.24) | copy-start | bytes 24580
Sparse Core Ops, SparseCore 0:
  9.4 66.9 all-gather.2
  78.6 49.9 all-gather.4
where the time goes:
time: 194 us
  blocking collectives  86.3 us (44%)
  matrix products  37.4 us (19%)
  waiting for transfers between devices  26.8 us (14%)
  between operations  13.7 us (7%)
  other arithmetic  13.2 us (7%)
  starting transfers between devices  8.21 us (4%)
  local copies, waits for them, and re-layouts  7.13 us (4%)
    all_to_all x2, blocking collectives, from_everyone(): lax.all_to_all(jnp.broadcast_to(value[None], (peers, *value.shape)), axis...  35.9 us
    all_to_all x1, blocking collectives, sum_by_axis(): lax.all_to_all(own.astype(jnp.bfloat16), far, 0, 0, tiled=True)  30.7 us
    all_gather x1, waiting for transfers between devices, on_device(): down_whole = lax.all_gather(contraction_matrix, 'sp', axis=1, tiled=True)  14.8 us
    dot_general x1, matrix products, on_device(): jnp.dot(hidden, down_whole, preferred_element_type=jnp.float32)  12.1 us
    all_to_all x1, blocking collectives, on_device(): lax.all_to_all(mixed, TP, split_axis=0, concat_axis=1, tiled=True)  11.6 us
    all_to_all x1, waiting for transfers between devices, from_everyone(): lax.all_to_all(jnp.broadcast_to(value[None], (peers, *value.shape)), axis...  11.2 us
    all_to_all x1, blocking collectives, summed_on_arrival(): lax.all_to_all(tiles, axis, split_axis=0, concat_axis=0, tiled=True)  8.18 us
    all_to_all x1, starting transfers between devices, from_everyone(): lax.all_to_all(jnp.broadcast_to(value[None], (peers, *value.shape)), axis...  8.16 us
  transfers between devices with their start and end apart: 3, of which 2 were waited for; matrix products, arithmetic and copies ran while one was open for 19% of the time, Pallas kernels for 0%

commit v1 on v0

--- a/solution.py
+++ b/solution.py
@@ -191,7 +191,11 @@
     contraction_matrix,
 ):
     gate_whole, up_whole = in_one_piece((switch_matrix, expansion_matrix), "sp", 0, 1)
-    down_whole = lax.all_gather(contraction_matrix, "sp", axis=1, tiled=True)
+    size = lax.axis_size("sp")
+    repeats = [size if d == 1 else 1 for d in range(contraction_matrix.ndim)]
+    down_whole = lax.all_to_all(
+        jnp.tile(contraction_matrix, repeats), "sp", split_axis=1, concat_axis=1, tiled=True
+    )
     heads_here = probe_preactivation.shape[1] // HEAD_DIM
     tok_rows = probe_preactivation.shape[0]
     arranged_sources = admission_source_matrix(

time: 194 us -> 221 us (1.14)
  waiting for transfers between devices: 26.8 us -> 44.4 us
  local copies, waits for them, and re-layouts: 7.13 us -> 11.8 us
  starting transfers between devices: 8.21 us -> 12.8 us
    all_to_all x0 -> x1, waiting for transfers between devices: none -> 32.4 us  [on_device(): lax.all_to_all(jnp.tile(contraction_matrix, repeats), 'sp', split_axis=1,...]
    all_gather x1 -> x0, waiting for transfers between devices: 14.8 us -> none  [on_device(): down_whole = lax.all_gather(contraction_matrix, 'sp', axis=1, tiled=True)]
    all_to_all x0 -> x1, starting transfers between devices: none -> 4.64 us  [on_device(): lax.all_to_all(jnp.tile(contraction_matrix, repeats), 'sp', split_axis=1,...]
    all_to_all x1, local copies, waits for them, and re-layouts: 2.33 us -> 4.8 us  [from_everyone(): lax.all_to_all(jnp.broadcast_to(value[None], (peers, *value.shape)), axis...]
where the time goes in v1:
time: 221 us; the launch traced here: 220 us
  blocking collectives  86.2 us (39%)
  waiting for transfers between devices  44.4 us (20%)
  matrix products  37.4 us (17%)
  between operations  13.7 us (6%)
  other arithmetic  13.1 us (6%)
  starting transfers between devices  12.8 us (6%)
  local copies, waits for them, and re-layouts  11.8 us (5%)
    all_to_all x2, blocking collectives, from_everyone(): lax.all_to_all(jnp.broadcast_to(value[None], (peers, *value.shape)), axis...  37 us
    all_to_all x1, waiting for transfers between devices, on_device(): lax.all_to_all(jnp.tile(contraction_matrix, repeats), 'sp', split_axis=1,...  32.4 us
    all_to_all x1, blocking collectives, sum_by_axis(): lax.all_to_all(own.astype(jnp.bfloat16), far, 0, 0, tiled=True)  29.4 us
    dot_general x1, matrix products, on_device(): jnp.dot(hidden, down_whole, preferred_element_type=jnp.float32)  12 us
    all_to_all x1, waiting for transfers between devices, from_everyone(): lax.all_to_all(jnp.broadcast_to(value[None], (peers, *value.shape)), axis...  12 us
    all_to_all x1, blocking collectives, on_device(): lax.all_to_all(mixed, TP, split_axis=0, concat_axis=1, tiled=True)  11.6 us
    all_to_all x1, blocking collectives, summed_on_arrival(): lax.all_to_all(tiles, axis, split_axis=0, concat_axis=0, tiled=True)  8.18 us
    all_to_all x1, starting transfers between devices, from_everyone(): lax.all_to_all(jnp.broadcast_to(value[None], (peers, *value.shape)), axis...  8.16 us
  transfers between devices with their start and end apart: 3, of which 2 were waited for; matrix products, arithmetic and copies ran while one was open for 19% of the time, Pallas kernels for 0%

profile of v1, /device:TPU:0, one launch (start us, length us, event | category | flops | bytes accessed | tf_op | source)
XLA Modules:
  0.0 220.4 jit_solution(11975222686143445894)
XLA Ops:
  6.5 1.8 pad_maximum_fusion
  8.4 1.1 convert_multiply_fusion.1
  9.5 1.0 convert.2
  10.5 1.4 divide_multiply_fusion
  11.9 17.0 %while.17 = (s32[]{:T(128)}, f32[1,128,128]{2,1,0:T(8,128)S(1)}, f32[1,128]{1,0:T(1,128)S(1)}, f32[16,1,64,128]{3,2,1,0:T(8,128)S(1)}, f32[16,1,64,128]{3,2,1,0:...) while((s32[]{:T(128)}, f32[1,128,128]{2,1,0:T(8,128)S(1)}, ...), condition=%wide.region_2.3_spmd.clone, body=%wide.region_0.2_spmd.clone.sunk | while | flops 38412544 | bytes 879768 | solution.py:209
  13.5 0.3 fusion.101
  14.6 0.3 fusion.101
  15.7 0.3 fusion.101
  16.7 0.3 fusion.101
  17.8 0.3 fusion.101
  18.9 0.3 fusion.101
  29.0 0.9 broadcast_in_dim.48
  29.9 8.2 %all-to-all-start = ((bf16[16,129,128]{2,1,0:T(8,128)(2,1)}), bf16[16,129,128]{2,1,0:T(8,128)(2,1)S(1)}, u32[]{:S(2)}, u32[]{:S(2)}) async-start(bf16[16,129,128]{2,1,0:T(8,128)(2,1)} %broadcast_in_dim.48), calls=%async_computation | async-start | bytes 1114112 | tf_op jit(solution)/shard_map/all_to_all | solution.py:26
  38.0 12.0 %all-to-all-done = bf16[16,129,128]{2,1,0:T(8,128)(2,1)S(1)} async-done(((bf16[16,129,128]{2,1,0:T(8,128)(2,1)}), bf16[16,129,128]{2,1,0:T(8,128)(2,1)S(1)}, u32[]{:S(2)}, u32[]{:S(2)}) %all-to-all-start) | async-done | bytes 528416 | tf_op jit(solution)/shard_map/all_to_all | solution.py:26
  50.8 0.7 multiply_reduce_fusion.1
  51.8 11.6 %all_to_all.53 = bf16[8,128,128]{2,1,0:T(8,128)(2,1)S(1)} all-to-all(bf16[8,128,128]{2,1,0:T(8,128)(2,1)S(1)} %bitcast.191), channel_id=1, replica_groups=mesh['sp'=16,'tp_0'=4,'tp_1'=2] {'tp_0','tp_1'}, dimensions={0} | all-to-all | bytes 524288 | tf_op jit(solution)/shard_map/all_to_all | solution.py:226
  63.6 3.0 %multiply_reduce_fusion = (f32[128]{0:T(128)S(1)}, f32[128,2048]{1,0:T(8,128)S(1)}) fusion(bf16[128,1024]{0,1:T(8,128)(2,1)S(1)} %bitcast.189, bf16[1024,2048]{1,0:T(8,128)(2,1)} %param.23, bf16[128,2048]{1,0:T(8,128)(2,1)S(1)} %copy-done), kind=kOutput, calls=%fused_computation.68 | convolution fusion | flops 538443648 | bytes 6029824 | tf_op jit(solution)/shard_map/dot_general | solution.py:227
  67.1 28.8 %all_to_all.54 = bf16[4,128,2048]{2,1,0:T(8,128)(2,1)S(1)} all-to-all(bf16[4,128,2048]{2,1,0:T(8,128)(2,1)S(1)} %broadcast_in_dim.74), channel_id=1, replica_groups=mesh['sp'=16,'tp_0'=4,'tp_1'=2] {'tp_0'}, dimensions={0} | all-to-all | bytes 4194304 | tf_op jit(solution)/shard_map/all_to_all | solution.py:26
  95.9 0.5 broadcast_in_dim.75
  96.4 8.3 %all_to_all.55 = bf16[2,4,128,2048]{3,2,1,0:T(8,128)(2,1)} all-to-all(bf16[2,4,128,2048]{3,2,1,0:T(8,128)(2,1)S(1)} %broadcast_in_dim.75), channel_id=1, replica_groups=mesh['sp'=16,'tp_0'=4,'tp_1'=2] {'tp_1'}, dimensions={0} | all-to-all | bytes 8388608 | tf_op jit(solution)/shard_map/all_to_all | solution.py:26
  104.7 2.2 tile.2
  106.8 4.6 %all-to-all-start.4 = ((bf16[704,16,128]{2,0,1:T(8,128)(2,1)}), bf16[704,16,128]{2,0,1:T(8,128)(2,1)}, u32[]{:S(2)}, u32[]{:S(2)}) async-start(bf16[704,16,128]{2,0,1:T(8,128)(2,1)} %tile.2), calls=%async_computation.4 | async-start | bytes 5767168 | tf_op jit(solution)/shard_map/all_to_all | solution.py:196
  111.5 4.8 %copy.45 = bf16[2,4,128,2048]{3,2,0,1:T(8,128)(2,1)} copy(bf16[2,4,128,2048]{3,2,1,0:T(8,128)(2,1)} %all_to_all.55) | data formatting | bytes 8388608 | tf_op jit(solution)/shard_map/all_to_all | solution.py:26
  116.3 7.8 %fusion.45 = f32[1024,704]{0,1:T(8,128)} fusion(bf16[1024,2048]{1,0:T(8,128)(2,1)} %bitcast.184, bf16[2048,1408]{0,1:T(8,128)(2,1)} %all-gather.2.cloned.1.call-done), kind=kOutput, calls=%fused_computation.58 | convolution fusion | flops 2952790016 | bytes 9961472 | tf_op jit(solution)/shard_map/dot_general | solution.py:231
  124.1 32.4 %all-to-all-done.4 = bf16[704,16,128]{2,0,1:T(8,128)(2,1)} async-done(((bf16[704,16,128]{2,0,1:T(8,128)(2,1)}), bf16[704,16,128]{2,0,1:T(8,128)(2,1)}, u32[]{:S(2)}, u32[]{:S(2)}) %all-to-all-start.4) | async-done | bytes 2883616 | tf_op jit(solution)/shard_map/all_to_all | solution.py:196
  156.6 12.0 %convolution_convert_fusion = bf16[1024,2048]{1,0:T(8,128)(2,1)} fusion(f32[1024,704]{0,1:T(8,128)} %fusion.45, bf16[1024,2048]{1,0:T(8,128)(2,1)} %bitcast.185, bf16[2048,1408]{0,1:T(8,128)(2,1)} %all-gather.2.cloned.1.call-done, bf16[704,16,128]{2,0,1:T(8,128)(2,1)} %all-to-all-done.4), kind=kOutput, calls=%fused_computation.53 | convolution fusion | flops 5912002560 | bytes 17039360 | tf_op jit(solution)/shard_map/dot_general | solution.py:234
  168.6 2.5 %copy.54 = bf16[4,2,128,2048]{3,2,0,1:T(8,128)(2,1)S(1)} copy(bf16[4,2,128,2048]{3,2,1,0:T(8,128)(2,1)} %bitcast.186) | data formatting | bytes 8388608 | tf_op jit(solution)/shard_map/reshape;reshape | solution.py:89
  171.1 8.2 %all_to_all.56 = bf16[2,4,128,2048]{3,2,1,0:T(8,128)(2,1)} all-to-all(bf16[2,4,128,2048]{3,2,1,0:T(8,128)(2,1)S(1)} %bitcast.183), channel_id=1, replica_groups=mesh['sp'=16,'tp_0'=4,'tp_1'=2] {'tp_1'}, dimensions={0} | all-to-all | bytes 8388608 | tf_op jit(solution)/shard_map/all_to_all | solution.py:95
  179.3 3.5 %reduce_sum.41 = bf16[4,128,2048]{2,1,0:T(8,128)(2,1)S(1)} reduce(bf16[2,4,128,2048]{3,2,1,0:T(8,128)(2,1)} %all_to_all.56, bf16[]{:T(256)} %constant.49.clone.1), dimensions={0}, to_apply=%region_5.6 | reduce | flops 1048576 | bytes 6291458 | tf_op jit(solution)/shard_map/reduce_sum | solution.py:96
  182.8 29.4 %all_to_all.57 = bf16[4,128,2048]{2,1,0:T(8,128)(2,1)S(1)} all-to-all(bf16[4,128,2048]{2,1,0:T(8,128)(2,1)S(1)} %reduce_sum.41), channel_id=1, replica_groups=mesh['sp'=16,'tp_0'=4,'tp_1'=2] {'tp_0'}, dimensions={0} | all-to-all | bytes 4194304 | tf_op jit(solution)/shard_map/all_to_all | solution.py:103
  212.2 0.4 convert_reduce_fusion
  212.6 0.9 add_convert_fusion
  (191 shorter events, 15.8 us)
Async XLA Ops:
  6.5 109.8 %all-gather.2.cloned.1.call-start = ((), (), s32[]{:S(2)}) async-start(), calls=%async_computation.7 | async-start | bytes 6127616 | tf_op jit(solution)/shard_map/all_gather | solution.py:17
  29.9 20.2 %all-to-all-start = ((bf16[16,129,128]{2,1,0:T(8,128)(2,1)}), bf16[16,129,128]{2,1,0:T(8,128)(2,1)S(1)}, u32[]{:S(2)}, u32[]{:S(2)}) async-start(bf16[16,129,128]{2,1,0:T(8,128)(2,1)} %broadcast_in_dim.48), calls=%async_computation | async-start | bytes 1114112 | tf_op jit(solution)/shard_map/all_to_all | solution.py:26
  50.2 1.5 copy-start.1
  50.2 1.4 copy-start.4
  50.5 13.1 %copy-start = (bf16[128,2048]{1,0:T(8,128)(2,1)S(1)}, bf16[128,2048]{1,0:T(8,128)(2,1)}, u32[]{:S(2)}) copy-start(bf16[128,2048]{1,0:T(8,128)(2,1)} %param.15) | copy-start | bytes 1572868
  63.6 3.0 %copy-start.3 = (f32[2048]{0:T(1024)S(1)}, f32[2048]{0:T(1024)}, u32[]{:S(2)}) copy-start(f32[2048]{0:T(1024)} %param.24) | copy-start | bytes 24580
  96.4 8.3 %copy-start.2 = (bf16[704,128]{1,0:T(8,128)(2,1)S(1)}, bf16[704,128]{1,0:T(8,128)(2,1)}, u32[]{:S(2)}) copy-start(bf16[704,128]{1,0:T(8,128)(2,1)} %param.27) | copy-start | bytes 540676
  106.8 49.7 %all-to-all-start.4 = ((bf16[704,16,128]{2,0,1:T(8,128)(2,1)}), bf16[704,16,128]{2,0,1:T(8,128)(2,1)}, u32[]{:S(2)}, u32[]{:S(2)}) async-start(bf16[704,16,128]{2,0,1:T(8,128)(2,1)} %tile.2), calls=%async_computation.4 | async-start | bytes 5767168 | tf_op jit(solution)/shard_map/all_to_all | solution.py:196
Sparse Core Ops, SparseCore 0:
  9.4 66.9 all-gather.1
